TPU v7x, 32 devices: a whole 2x2x4 slice. The times are simulated.
32 devices in a mesh: sp: 8 (over z, core), tp: 4 (over y, x).
Axes of the slice: x: 2, y: 2, z: 4, core: 2. Of those that a mesh axis runs over, the one named last changes fastest.
Arguments:
- moe_input: bfloat16 [1024, 2048], P('sp', 'tp'), may hold values from -6 to 6
- cotangent: bfloat16 [1024, 2048], P('sp', 'tp'), may hold values from -6 to 6
- routes: int32 [1024, 2], P('sp'), may hold values from 0 to 7, all different within a row; in each aligned block of 128 rows (0 to 127, 128 to 255, ...) at most 64 rows name the same one
- route_weight: float32 [1024, 2], P('sp'), may hold values from 0.1 to 1
- w_gate: bfloat16 [8, 2816, 2048], P('sp', 'tp'), may hold values from -0.125 to 0.125
- w_up: bfloat16 [8, 2816, 2048], P('sp', 'tp'), may hold values from -0.125 to 0.125
- w_down: bfloat16 [8, 2816, 2048], P('sp', 'tp'), may hold values from -0.109375 to 0.109375
- v_value: bfloat16 [1024, 1024], P('sp', 'tp'), may hold values from -6 to 6
- v_gate: bfloat16 [1024, 1024], P('sp', 'tp'), may hold values from -12 to 12
- conv_out: bfloat16 [1024, 1024], P('sp', 'tp'), may hold values from -6 to 6
- row_mean: float32 [1024], P('sp'), may hold values from -3 to 3
- row_rstd: float32 [1024], P('sp'), may hold values from 0.5 to 2
- ln_gain: float32 [1024], P('tp'), may hold values from 0.1 to 1.9
- taps: bfloat16 [31, 1024], P(None, 'tp'), may hold values from -1 to 1
- out_proj: bfloat16 [2048, 1024], P('sp', 'tp'), may hold values from -0.1875 to 0.1875
Outputs:
- gate_grad: bfloat16 [8, 2816, 2048], P('sp', 'tp')
- up_grad: bfloat16 [8, 2816, 2048], P('sp', 'tp')
- down_grad: bfloat16 [8, 2816, 2048], P('sp', 'tp')
- proj_grad: float32 [2048, 1024], P('sp', 'tp')
- stream_grad: bfloat16 [1024, 2048], P('sp', 'tp')
- value_grad: bfloat16 [1024, 1024], P('sp', 'tp')
- gating_grad: bfloat16 [1024, 1024], P('sp', 'tp')
Inputs may be any that keep to these rules, and one draw needn't show every extreme that they name: `routes`: in the rows of one device no expert is named more than 64 times.
All inputs are finite; a program needn't handle non-finite values.
Results may differ from a plain program's by a relative error of at most 0.025.
Values may be sent and summed in bfloat16 or wider, within the bound.
A program may use at most 64 MiB of HBM per device.

v0:
```python
import jax
import jax.numpy as jnp
from jax import lax
from jax.sharding import PartitionSpec as P


def passed_along(value, axis, steps):
    count = lax.axis_size(axis)
    leading, last = (max(0, -steps), min(count, count - steps))
    return lax.ppermute(value, axis, [(source, source + steps) for source in range(leading, last)])


def route_targets(routes, experts, capacity):
    flat_routes = routes.reshape(-1)
    member = (flat_routes[:, None] == jnp.arange(experts, dtype=jnp.int32)[None, :]).astype(
        jnp.int32
    )
    earlier = jnp.cumsum(member, axis=0) - member
    slot_index = jnp.sum(earlier * member, axis=1)
    return flat_routes * capacity + slot_index


def contract_rows(left, right):
    return lax.dot_general(
        left, right, (((0,), (0,)), ((), ())), preferred_element_type=jnp.float32
    )


def contract_cols(left, right):
    return lax.dot_general(
        left, right, (((1,), (1,)), ((), ())), preferred_element_type=jnp.float32
    )


def shards(
    moe_input,
    cotangent,
    routes,
    route_weight,
    w_gate,
    w_up,
    w_down,
    v_value,
    v_gate,
    conv_out,
    row_mean,
    row_rstd,
    ln_gain,
    taps,
    out_proj,
):
    experts = lax.axis_size("sp")
    tokens = routes.shape[0]
    capacity = 4 * tokens // experts
    total = experts * capacity
    buffer_row = route_targets(routes, experts, capacity)
    token_index = jnp.arange(2 * tokens, dtype=jnp.int32) // 2
    weights = route_weight.reshape(-1)
    width = moe_input.shape[1]
    picked = moe_input[token_index]
    weighted = (weights[:, None] * cotangent[token_index].astype(jnp.float32)).astype(jnp.bfloat16)
    rows_buf = jnp.zeros((total, width), jnp.bfloat16).at[buffer_row].set(picked)
    cotan_buf = jnp.zeros((total, width), jnp.bfloat16).at[buffer_row].set(weighted)
    rows_buf, cotan_buf = (
        rows_buf.reshape(experts, capacity, width),
        cotan_buf.reshape(experts, capacity, width),
    )
    part_rows, part_cotan = (
        lax.all_to_all(rows_buf, "sp", split_axis=0, concat_axis=0, tiled=True),
        lax.all_to_all(cotan_buf, "sp", split_axis=0, concat_axis=0, tiled=True),
    )
    arrived_rows, arrived_cotan = (
        lax.all_gather(part_rows, "tp", axis=2, tiled=True),
        lax.all_gather(part_cotan, "tp", axis=2, tiled=True),
    )
    width = arrived_rows.shape[2]
    expert_in = arrived_rows.reshape(total, width)
    expert_cot = arrived_cotan.reshape(total, width)
    gate_w = w_gate[0]
    up_w = w_up[0]
    down_w = w_down[0]
    gate_pre = contract_cols(expert_in, gate_w)
    up_pre = contract_cols(expert_in, up_w)
    gate_sig = jax.nn.sigmoid(gate_pre)
    gate_act = gate_pre * gate_sig
    hidden = (gate_act * up_pre).astype(jnp.bfloat16)
    down_g = contract_rows(hidden, expert_cot).astype(jnp.bfloat16)
    hidden_grad = contract_cols(expert_cot, down_w)
    gate_delta = (hidden_grad * up_pre * gate_sig * (1.0 + gate_pre * (1.0 - gate_sig))).astype(
        jnp.bfloat16
    )
    up_delta = (hidden_grad * gate_act).astype(jnp.bfloat16)
    gate_g = contract_rows(gate_delta, expert_in).astype(jnp.bfloat16)
    up_g = contract_rows(up_delta, expert_in).astype(jnp.bfloat16)
    partial_value = jnp.dot(gate_delta, gate_w, preferred_element_type=jnp.float32) + jnp.dot(
        up_delta, up_w, preferred_element_type=jnp.float32
    )
    row_share = lax.psum_scatter(
        partial_value.astype(jnp.bfloat16), "tp", scatter_dimension=1, tiled=True
    )
    slice_width = row_share.shape[1]
    returned = lax.all_to_all(
        row_share.reshape(experts, capacity, slice_width),
        "sp",
        split_axis=0,
        concat_axis=0,
        tiled=True,
    )
    mine = (
        returned.reshape(total, slice_width)[buffer_row]
        .astype(jnp.float32)
        .reshape(tokens, 2, slice_width)
    )
    stream = (cotangent.astype(jnp.float32) + (mine[:, 0] + mine[:, 1])).astype(jnp.bfloat16)
    full_stream = lax.all_gather(stream, "tp", axis=1, tiled=True)
    normed = (conv_out.astype(jnp.float32) - row_mean[:, None]) * row_rstd[:, None]
    scaled_norm = normed * ln_gain[None, :]
    norm_sig = jax.nn.sigmoid(scaled_norm)
    mixed = (scaled_norm * norm_sig).astype(jnp.bfloat16)
    columns = full_stream
    mixed_grad = jnp.dot(
        columns,
        lax.all_gather(out_proj, "sp", axis=0, tiled=True),
        preferred_element_type=jnp.float32,
    )
    columns = full_stream
    proj_g = lax.psum_scatter(
        contract_rows(columns, mixed).astype(jnp.bfloat16), "sp", scatter_dimension=0, tiled=True
    ).astype(jnp.float32)
    channels = out_proj.shape[1] * lax.axis_size("tp")
    norm_grad = mixed_grad * norm_sig * (1.0 + scaled_norm * (1.0 - norm_sig)) * ln_gain[None, :]
    first_sum, second_sum = lax.psum(
        (jnp.sum(norm_grad, axis=1), jnp.sum(norm_grad * normed, axis=1)), "tp"
    )
    first_mean = first_sum[:, None] / channels
    second_mean = second_sum[:, None] / channels
    conv_grad = row_rstd[:, None] * (norm_grad - first_mean - normed * second_mean)
    kernel = taps.shape[0]
    following = passed_along(conv_grad[: kernel - 1], "sp", -1)
    extended = jnp.concatenate([conv_grad, following], axis=0)
    tap_values = taps.astype(jnp.float32)
    unit_grad = jnp.zeros_like(conv_grad)
    for offset in range(kernel):
        lead = kernel - 1 - offset
        unit_grad = unit_grad + tap_values[offset][None, :] * extended[lead : lead + tokens]
    value_sig = jax.nn.sigmoid(v_gate.astype(jnp.float32))
    value_g = (unit_grad * value_sig).astype(jnp.bfloat16)
    gating_g = (unit_grad * v_value.astype(jnp.float32) * value_sig * (1.0 - value_sig)).astype(
        jnp.bfloat16
    )
    return (gate_g[None], up_g[None], down_g[None], proj_g, stream, value_g, gating_g)


def solution(mesh):
    return jax.shard_map(
        shards,
        mesh=mesh,
        in_specs=(
            P("sp", "tp"),
            P("sp", "tp"),
            P("sp", None),
            P("sp", None),
            P("sp", "tp", None),
            P("sp", "tp", None),
            P("sp", "tp", None),
            P("sp", "tp"),
            P("sp", "tp"),
            P("sp", "tp"),
            P("sp"),
            P("sp"),
            P("tp"),
            P(None, "tp"),
            P("sp", "tp"),
        ),
        out_specs=(
            P("sp", "tp", None),
            P("sp", "tp", None),
            P("sp", "tp", None),
            P("sp", "tp"),
            P("sp", "tp"),
            P("sp", "tp"),
            P("sp", "tp"),
        ),
        check_vma=False,
    )
```

profile of v0, /device:TPU:0, one launch (start us, length us, event | category | flops | bytes accessed | tf_op | source)
XLA Modules:
  0.0 229.9 jit_solution(8924655824834304868)
XLA Ops:
  8.1 0.9 copy.25
  9.3 0.7 broadcast_multiply_fusion
  11.2 3.9 %scatter_custom_fusion.1 = bf16[512,512]{1,0:T(8,128)(2,1)S(1)} fusion(s32[256]{0:T(256)S(1)} %bitcast.123, bf16[128,512]{1,0:T(8,128)(2,1)} %param.15, s32[1024]{0:T(1024)S(1)} %pad_clamp_fusion.1, bf16[]{:T(256)} %constant.29.clone.1), kind=kCustom, calls=%fused_computation.94 | custom fusion | bytes 524800 | tf_op jit(solution)/shard_map/scatter | solution.py:62
  15.1 21.6 %all_to_all.15 = bf16[8,64,512]{2,1,0:T(8,128)(2,1)} all-to-all(bf16[8,64,512]{2,1,0:T(8,128)(2,1)S(1)} %bitcast.90), channel_id=1, replica_groups=mesh['sp'=8,'tp'=4] {'sp'}, dimensions={0} | all-to-all | bytes 1048576 | tf_op jit(solution)/shard_map/all_to_all | solution.py:69
  37.1 2.9 %scatter_custom_fusion = bf16[512,512]{1,0:T(8,128)(2,1)S(1)} fusion(s32[256]{0:T(256)S(1)} %bitcast.124, f32[256]{0:T(256)S(1)} %mul.427, bf16[]{:T(256)} %constant.29.clone.1, bf16[128,512]{1,0:T(8,128)(2,1)S(1)} %copy-done.3, s32[1024]{0:T(1024)S(1)} %pad_clamp_fusion.1), kind=kCustom, calls=%fused_computation.89 | custom fusion | flops 393216 | bytes 660482 | tf_op jit(solution)/shard_map/scatter | solution.py:63
  39.9 18.4 %all_to_all.16 = bf16[8,64,512]{2,1,0:T(8,128)(2,1)} all-to-all(bf16[8,64,512]{2,1,0:T(8,128)(2,1)S(1)} %bitcast.89), channel_id=1, replica_groups=mesh['sp'=8,'tp'=4] {'sp'}, dimensions={0} | all-to-all | bytes 1048576 | tf_op jit(solution)/shard_map/all_to_all | solution.py:70
  58.6 12.3 %all-gather.6.cloned.1.call-done = bf16[8,64,2048]{2,1,0:T(8,128)(2,1)} async-done(((bf16[8,64,512]{2,1,0:T(8,128)(2,1)}), bf16[8,64,2048]{2,1,0:T(8,128)(2,1)}) %all-gather.6.cloned.1.call-update) | async-done | bytes 2097168 | tf_op jit(solution)/shard_map/all_gather | solution.py:73
  70.9 4.5 %fusion.5 = f32[512,704]{0,1:T(8,128)} fusion(bf16[512,2048]{1,0:T(8,128)(2,1)} %bitcast.128, bf16[1,704,2048]{2,1,0:T(8,128)(2,1)S(1)} %copy-done), kind=kOutput, calls=%fused_computation.14 | convolution fusion | flops 1476395008 | bytes 6422528 | tf_op jit(solution)/shard_map/dot_general | solution.py:30
  75.4 2.8 %fusion.8 = f32[512,704]{0,1:T(8,128)} fusion(bf16[512,2048]{1,0:T(8,128)(2,1)S(1)} %bitcast.131, bf16[1,704,2048]{2,1,0:T(8,128)(2,1)S(1)} %copy-done.42), kind=kOutput, calls=%fused_computation.17 | convolution fusion | flops 1476395008 | bytes 6422528 | tf_op jit(solution)/shard_map/dot_general | solution.py:30
  78.2 29.5 %all-gather.4.cloned.1.call-done = bf16[8,64,2048]{2,1,0:T(8,128)(2,1)} async-done(((bf16[8,64,512]{2,1,0:T(8,128)(2,1)}), bf16[8,64,2048]{2,1,0:T(8,128)(2,1)}) %all-gather.4.cloned.1.call-update) | async-done | bytes 2097168 | tf_op jit(solution)/shard_map/all_gather | solution.py:74
  107.8 5.4 %multiply_convert_fusion.1 = (bf16[512,704]{0,1:T(8,128)(2,1)S(1)}, bf16[512,704]{0,1:T(8,128)(2,1)S(1)}) fusion(f32[512,704]{0,1:T(8,128)} %fusion.5, f32[512,704]{0,1:T(8,128)} %fusion.8, bf16[512,2048]{1,0:T(8,128)(2,1)} %bitcast.132, bf16[1,704,2048]{2,1,0:T(8,128)(2,1)} %param.21), kind=kOutput, calls=%fused_computation.52 | convolution fusion | flops 1481080832 | bytes 9306112 | tf_op jit(solution)/shard_map/dot_general | solution.py:30
  113.2 1.9 fusion.3
  115.5 3.3 %add_convert_fusion = bf16[512,2048]{1,0:T(8,128)(2,1)} fusion(f32[512,2048]{1,0:T(8,128)S(1)} %fusion.3, bf16[512,704]{0,1:T(8,128)(2,1)S(1)} %get-tuple-element.13, bf16[1,704,2048]{2,1,0:T(8,128)(2,1)S(1)} %copy-done.43), kind=kOutput, calls=%fused_computation.5 | convolution fusion | flops 1478492160 | bytes 9895936 | tf_op jit(solution)/shard_map/dot_general | solution.py:95
  119.4 34.8 %reduce-scatter.3.cloned.1.call-done = bf16[512,512]{1,0:T(8,128)(2,1)} async-done(((bf16[512,2048]{1,0:T(8,128)(2,1)}), bf16[512,512]{1,0:T(8,128)(2,1)}) %reduce-scatter.3.cloned.1.call-update) | async-done | bytes 524304 | tf_op jit(solution)/shard_map/reduce_scatter | solution.py:98
  154.2 4.6 %all-to-all-start.2 = ((bf16[8,64,512]{2,1,0:T(8,128)(2,1)}), bf16[8,64,512]{2,1,0:T(8,128)(2,1)S(1)}, u32[]{:S(2)}, u32[]{:S(2)}) async-start(bf16[8,64,512]{2,1,0:T(8,128)(2,1)} %bitcast.91), calls=%async_computation.3 | async-start | bytes 1048576 | tf_op jit(solution)/shard_map/all_to_all | solution.py:102
  160.2 5.1 %fusion.1 = bf16[1,704,2048]{2,1,0:T(8,128)(2,1)} fusion(bf16[512,704]{0,1:T(8,128)(2,1)} %copy-done.45, bf16[512,2048]{1,0:T(8,128)(2,1)} %bitcast.129), kind=kOutput, calls=%fused_computation.10 | convolution fusion | flops 1477836800 | bytes 5701632 | tf_op jit(solution)/shard_map/dot_general | solution.py:24
  165.2 8.9 %all-to-all-done.2 = bf16[8,64,512]{2,1,0:T(8,128)(2,1)S(1)} async-done(((bf16[8,64,512]{2,1,0:T(8,128)(2,1)}), bf16[8,64,512]{2,1,0:T(8,128)(2,1)S(1)}, u32[]{:S(2)}, u32[]{:S(2)}) %all-to-all-start.2) | async-done | bytes 524320 | tf_op jit(solution)/shard_map/all_to_all | solution.py:102
  174.1 1.9 gather_fusion
  176.0 1.3 reshape.141
  177.7 1.0 fusion.18
  178.7 10.5 %all_gather.14 = bf16[128,2048]{1,0:T(8,128)(2,1)S(1)} all-gather(bf16[128,512]{1,0:T(8,128)(2,1)S(1)} %fusion.18), channel_id=1, replica_groups=mesh['sp'=8,'tp'=4] {'tp'}, dimensions={1}, use_global_device_ids=true | all-gather | bytes 655360 | tf_op jit(solution)/shard_map/all_gather | solution.py:115
  189.2 1.6 convolution_convert_fusion.3
  190.8 5.7 %fusion.2 = bf16[1,704,2048]{2,1,0:T(8,128)(2,1)} fusion(bf16[512,2048]{1,0:T(8,128)(2,1)} %bitcast.133, f32[512,704]{0,1:T(8,128)} %fusion.8, f32[512,704]{0,1:T(8,128)} %fusion.5), kind=kOutput, calls=%fused_computation.11 | convolution fusion | flops 1479999488 | bytes 7864320 | tf_op jit(solution)/shard_map/dot_general | solution.py:24
  196.6 2.3 fusion.125
  198.9 8.9 %all-reduce = (f32[128]{0:T(128)S(1)}, f32[128]{0:T(128)S(1)}) all-reduce(f32[128]{0:T(128)S(1)} %get-tuple-element.8, f32[128]{0:T(128)S(1)} %get-tuple-element.7), channel_id=1, replica_groups=mesh['sp'=8,'tp'=4] {'tp'}, use_global_device_ids=true, to_apply=%region_10.11 | all-reduce | flops 256 | bytes 2048 | tf_op jit(solution)/shard_map/psum | solution.py:132
  207.8 1.0 subtract_multiply_fusion
  209.2 1.3 collective-permute-start
  210.5 5.1 %fusion = bf16[1,704,2048]{2,1,0:T(8,128)(2,1)} fusion(bf16[512,704]{0,1:T(8,128)(2,1)} %copy-done.1, bf16[512,2048]{1,0:T(8,128)(2,1)} %bitcast.130), kind=kOutput, calls=%fused_computation.9 | convolution fusion | flops 1477836800 | bytes 5701632 | tf_op jit(solution)/shard_map/dot_general | solution.py:24
  215.8 1.1 multiply_convert_fusion.6
  217.0 0.7 multiply_convert_fusion.7
  217.6 3.5 %reduce-scatter.5.cloned.1.call-done = bf16[256,256]{1,0:T(8,128)(2,1)} async-done(((bf16[2048,256]{1,0:T(8,128)(2,1)}), bf16[256,256]{1,0:T(8,128)(2,1)}) %reduce-scatter.5.cloned.1.call-update) | async-done | bytes 131088 | tf_op jit(solution)/shard_map/reduce_scatter | solution.py:127
  221.1 1.6 convert_element_type.92
  (125 shorter events, 5.1 us)
Async XLA Ops:
  8.0 62.9 %copy-start = (bf16[1,704,2048]{2,1,0:T(8,128)(2,1)S(1)}, bf16[1,704,2048]{2,1,0:T(8,128)(2,1)}, u32[]{:S(2)}) copy-start(bf16[1,704,2048]{2,1,0:T(8,128)(2,1)} %param.19) | copy-start | bytes 8650756
  8.0 28.8 %copy-start.40 = (f32[128,2]{0,1:T(2,128)S(1)}, f32[128,2]{0,1:T(2,128)}, u32[]{:S(2)}) copy-start(f32[128,2]{0,1:T(2,128)} %param.18) | copy-start | bytes 3076
  8.0 29.0 %copy-start.3 = (bf16[128,512]{1,0:T(8,128)(2,1)S(1)}, bf16[128,512]{1,0:T(8,128)(2,1)}, u32[]{:S(2)}) copy-start(bf16[128,512]{1,0:T(8,128)(2,1)} %param.16) | copy-start | bytes 393220
  8.0 62.8 %all-gather.6.cloned.1.call-start = ((), (), s32[]{:S(2)}) async-start(), calls=%async_computation.6 | async-start | bytes 2621440 | tf_op jit(solution)/shard_map/all_gather | solution.py:73
  36.7 71.0 %all-gather.4.cloned.1.call-start = ((), (), s32[]{:S(2)}) async-start(), calls=%async_computation.5 | async-start | bytes 2621440 | tf_op jit(solution)/shard_map/all_gather | solution.py:74
  58.4 95.8 %reduce-scatter.3.cloned.1.call-start = ((), (), s32[]{:S(2)}) async-start(), calls=%async_computation.7 | async-start | bytes 2621440 | tf_op jit(solution)/shard_map/reduce_scatter | solution.py:98
  118.8 40.0 %copy-start.8 = (bf16[31,256]{1,0:T(8,128)(2,1)S(1)}, bf16[31,256]{1,0:T(8,128)(2,1)}, u32[]{:S(2)}) copy-start(bf16[31,256]{1,0:T(8,128)(2,1)} %param.28) | copy-start | bytes 47620
  118.8 77.7 %all-gather.8.cloned.1.call-start = ((), (), s32[]{:S(2)}) async-start(), calls=%async_computation.9 | async-start | bytes 1179648 | tf_op jit(solution)/shard_map/all_gather | solution.py:123
  154.2 19.9 %all-to-all-start.2 = ((bf16[8,64,512]{2,1,0:T(8,128)(2,1)}), bf16[8,64,512]{2,1,0:T(8,128)(2,1)S(1)}, u32[]{:S(2)}, u32[]{:S(2)}) async-start(bf16[8,64,512]{2,1,0:T(8,128)(2,1)} %bitcast.91), calls=%async_computation.3 | async-start | bytes 1048576 | tf_op jit(solution)/shard_map/all_to_all | solution.py:102
  158.8 62.3 %reduce-scatter.5.cloned.1.call-start = ((), (), s32[]{:S(2)}) async-start(), calls=%async_computation.8 | async-start | bytes 1179648 | tf_op jit(solution)/shard_map/reduce_scatter | solution.py:127
  177.3 11.9 %copy-start.4 = (bf16[128,256]{1,0:T(8,128)(2,1)S(1)}, bf16[128,256]{1,0:T(8,128)(2,1)}, u32[]{:S(2)}) copy-start(bf16[128,256]{1,0:T(8,128)(2,1)} %param.24) | copy-start | bytes 196612
  177.3 11.9 %copy-start.36 = (f32[128]{0:T(128)S(1)}, f32[128]{0:T(128)}, u32[]{:S(2)}) copy-start(f32[128]{0:T(128)} %param.26) | copy-start | bytes 1540
  177.3 11.9 %copy-start.38 = (f32[128]{0:T(128)S(1)}, f32[128]{0:T(128)}, u32[]{:S(2)}) copy-start(f32[128]{0:T(128)} %param.25) | copy-start | bytes 1540
  177.3 11.9 %copy-start.41 = (f32[256]{0:T(256)S(1)}, f32[256]{0:T(256)}, u32[]{:S(2)}) copy-start(f32[256]{0:T(256)} %param.27) | copy-start | bytes 3076
  178.7 17.9 %copy-start.2 = (bf16[128,512]{1,0:T(8,128)(2,1)}, bf16[128,512]{1,0:T(8,128)(2,1)S(1)}, u32[]{:S(2)}) copy-start(bf16[128,512]{1,0:T(8,128)(2,1)S(1)} %fusion.18) | copy-start | bytes 393220
  196.6 11.2 %copy-start.5 = (bf16[128,256]{1,0:T(8,128)(2,1)S(1)}, bf16[128,256]{1,0:T(8,128)(2,1)}, u32[]{:S(2)}) copy-start(bf16[128,256]{1,0:T(8,128)(2,1)} %param.24) | copy-start | bytes 196612
  196.6 11.2 %copy-start.37 = (f32[128]{0:T(128)S(1)}, f32[128]{0:T(128)}, u32[]{:S(2)}) copy-start(f32[128]{0:T(128)} %param.26) | copy-start | bytes 1540
  196.6 11.2 %copy-start.39 = (f32[128]{0:T(128)S(1)}, f32[128]{0:T(128)}, u32[]{:S(2)}) copy-start(f32[128]{0:T(128)} %param.25) | copy-start | bytes 1540
  208.9 6.7 %copy-start.6 = (bf16[128,256]{1,0:T(8,128)(2,1)S(1)}, bf16[128,256]{1,0:T(8,128)(2,1)}, u32[]{:S(2)}) copy-start(bf16[128,256]{1,0:T(8,128)(2,1)} %param.23) | copy-start | bytes 196612
  208.9 6.7 %copy-start.7 = (bf16[128,256]{1,0:T(8,128)(2,1)S(1)}, bf16[128,256]{1,0:T(8,128)(2,1)}, u32[]{:S(2)}) copy-start(bf16[128,256]{1,0:T(8,128)(2,1)} %param.22) | copy-start | bytes 196612
  208.9 6.7 %copy-start.9 = (f32[1,256]{1,0:T(1,128)S(1)}, f32[1,256]{1,0:T(1,128)}, u32[]{:S(2)}) copy-start(f32[1,256]{1,0:T(1,128)} %get-tuple-element.40) | copy-start | bytes 3076
  208.9 6.7 %copy-start.10 = (f32[1,256]{1,0:T(1,128)S(1)}, f32[1,256]{1,0:T(1,128)}, u32[]{:S(2)}) copy-start(f32[1,256]{1,0:T(1,128)} %get-tuple-element.41) | copy-start | bytes 3076
  208.9 6.6 %copy-start.11 = (f32[1,256]{1,0:T(1,128)S(1)}, f32[1,256]{1,0:T(1,128)}, u32[]{:S(2)}) copy-start(f32[1,256]{1,0:T(1,128)} %get-tuple-element.42) | copy-start | bytes 3076
  208.9 6.6 %copy-start.12 = (f32[1,256]{1,0:T(1,128)S(1)}, f32[1,256]{1,0:T(1,128)}, u32[]{:S(2)}) copy-start(f32[1,256]{1,0:T(1,128)} %get-tuple-element.43) | copy-start | bytes 3076
  208.9 6.6 %copy-start.13 = (f32[1,256]{1,0:T(1,128)S(1)}, f32[1,256]{1,0:T(1,128)}, u32[]{:S(2)}) copy-start(f32[1,256]{1,0:T(1,128)} %get-tuple-element.44) | copy-start | bytes 3076
  208.9 6.6 %copy-start.14 = (f32[1,256]{1,0:T(1,128)S(1)}, f32[1,256]{1,0:T(1,128)}, u32[]{:S(2)}) copy-start(f32[1,256]{1,0:T(1,128)} %get-tuple-element.45) | copy-start | bytes 3076
  209.0 6.6 %copy-start.15 = (f32[1,256]{1,0:T(1,128)S(1)}, f32[1,256]{1,0:T(1,128)}, u32[]{:S(2)}) copy-start(f32[1,256]{1,0:T(1,128)} %get-tuple-element.46) | copy-start | bytes 3076
  209.0 6.6 %copy-start.16 = (f32[1,256]{1,0:T(1,128)S(1)}, f32[1,256]{1,0:T(1,128)}, u32[]{:S(2)}) copy-start(f32[1,256]{1,0:T(1,128)} %get-tuple-element.47) | copy-start | bytes 3076
  209.0 6.6 %copy-start.17 = (f32[1,256]{1,0:T(1,128)S(1)}, f32[1,256]{1,0:T(1,128)}, u32[]{:S(2)}) copy-start(f32[1,256]{1,0:T(1,128)} %get-tuple-element.17) | copy-start | bytes 3076
  209.0 6.6 %copy-start.18 = (f32[1,256]{1,0:T(1,128)S(1)}, f32[1,256]{1,0:T(1,128)}, u32[]{:S(2)}) copy-start(f32[1,256]{1,0:T(1,128)} %get-tuple-element.18) | copy-start | bytes 3076
  209.0 6.6 %copy-start.19 = (f32[1,256]{1,0:T(1,128)S(1)}, f32[1,256]{1,0:T(1,128)}, u32[]{:S(2)}) copy-start(f32[1,256]{1,0:T(1,128)} %get-tuple-element.19) | copy-start | bytes 3076
  209.2 6.4 %collective-permute-start = (f32[30,256]{1,0:T(8,128)S(1)}, f32[30,256]{1,0:T(8,128)S(1)}, u32[]{:S(2)}, u32[]{:S(2)}) collective-permute-start(f32[30,256]{1,0:T(8,128)S(1)} %slice.274), channel_id=1, source_target_pairs={{4,0},{8,4},{12,8},{16,12},{20,16},{24,20},{28,24},{5,1},{9,5},{13... | collective-permute-start | bytes 92168 | tf_op jit(solution)/shard_map/ppermute | solution.py:10
  (21 other events, 121.6 us)
Sparse Core Ops, SparseCore 0:
  36.9 33.9 all-gather.5
  72.7 35.0 all-gather.3
  119.0 35.1 reduce-scatter.2
Sparse Core Ops, SparseCore 1:
  120.9 22.1 all-gather.7
  190.9 30.2 reduce-scatter.4
where the time goes:
time: 231 us; the launch traced here: 230 us
  waiting for transfers between devices  89.5 us (39%)
  blocking collectives  59.4 us (26%)
  matrix products  37.7 us (16%)
  between operations  15.9 us (7%)
  local copies, waits for them, and re-layouts  11.3 us (5%)
  other arithmetic  9.76 us (4%)
  starting transfers between devices  6.28 us (3%)
    reduce_scatter x1, waiting for transfers between devices, shards(): lax.psum_scatter(partial_value.astype(jnp.bfloat16), 'tp', scatter_dimens...  34.8 us
    all_gather x1, waiting for transfers between devices, shards(): lax.all_gather(part_cotan, 'tp', axis=2, tiled=True)  29.5 us
    all_to_all x1, blocking collectives, shards(): lax.all_to_all(rows_buf, 'sp', split_axis=0, concat_axis=0, tiled=True)  21.6 us
    all_to_all x1, blocking collectives, shards(): lax.all_to_all(cotan_buf, 'sp', split_axis=0, concat_axis=0, tiled=True)  18.4 us
    dot_general x4, matrix products, contract_rows(): lax.dot_general(left, right, (((0,), (0,)), ((), ())), preferred_element_...  17.5 us
    dot_general x3, matrix products, contract_cols(): lax.dot_general(left, right, (((1,), (1,)), ((), ())), preferred_element_...  12.7 us
    all_gather x1, waiting for transfers between devices, shards(): lax.all_gather(part_rows, 'tp', axis=2, tiled=True)  12.3 us
    all_gather x1, blocking collectives, shards(): full_stream = lax.all_gather(stream, 'tp', axis=1, tiled=True)  10.5 us
  transfers between devices with their start and end apart: 7, of which 5 were waited for; matrix products, arithmetic and copies ran while one was open for 17% of the time, Pallas kernels for 0%

commit v1 on v0

--- a/solution.py
+++ b/solution.py
@@ -2,6 +2,11 @@
 import jax.numpy as jnp
 from jax import lax
 from jax.sharding import PartitionSpec as P
+
+
+def gather_over(x, name, d):
+    sent = jnp.stack([x] * lax.axis_size(name))
+    return jnp.concatenate(lax.all_to_all(sent, name, 0, 0), axis=d)
 
 
 def passed_along(value, axis, steps):
@@ -71,7 +76,7 @@
     )
     arrived_rows, arrived_cotan = (
         lax.all_gather(part_rows, "tp", axis=2, tiled=True),
-        lax.all_gather(part_cotan, "tp", axis=2, tiled=True),
+        gather_over(part_cotan, "tp", 2),
     )
     width = arrived_rows.shape[2]
     expert_in = arrived_rows.reshape(total, width)

time: 231 us -> 223 us (0.965)
  waiting for transfers between devices: 89.5 us -> 47.1 us
  blocking collectives: 59.4 us -> 94.2 us
  matrix products: 37.7 us -> 32.2 us
  local copies, waits for them, and re-layouts: 11.3 us -> 16.4 us
    all_to_all x0 -> x1, blocking collectives: none -> 35.7 us  [gather_over(): return jnp.concatenate(lax.all_to_all(sent, name, 0, 0), axis=d)]
    all_gather x1 -> x0, waiting for transfers between devices: 29.5 us -> none  [shards(): lax.all_gather(part_cotan, 'tp', axis=2, tiled=True)]
    all_gather x1, waiting for transfers between devices: 12.3 us -> 0.01 us  [shards(): lax.all_gather(part_rows, 'tp', axis=2, tiled=True)]
    dot_general x3, matrix products: 12.7 us -> 7.24 us  [contract_cols(): lax.dot_general(left, right, (((1,), (1,)), ((), ())), preferred_element_...]
    unnamed x94 -> x101, local copies, waits for them, and re-layouts: 1.69 us -> 4.98 us
  transfers between devices with their start and end apart: 7 -> 6, of which waited for: 5 -> 3; matrix products, arithmetic and copies ran while one was open for 17% -> 16% of each run, Pallas kernels for 0% -> 0%
where the time goes in v1:
time: 223 us; the launch traced here: 222 us
  blocking collectives  94.2 us (42%)
  waiting for transfers between devices  47.1 us (21%)
  matrix products  32.2 us (14%)
  local copies, waits for them, and re-layouts  16.4 us (7%)
  between operations  16.3 us (7%)
  other arithmetic  9.76 us (4%)
  starting transfers between devices  6.26 us (3%)
    all_to_all x1, blocking collectives, gather_over(): return jnp.concatenate(lax.all_to_all(sent, name, 0, 0), axis=d)  35.7 us
    reduce_scatter x1, waiting for transfers between devices, shards(): lax.psum_scatter(partial_value.astype(jnp.bfloat16), 'tp', scatter_dimens...  34.2 us
    all_to_all x1, blocking collectives, shards(): lax.all_to_all(rows_buf, 'sp', split_axis=0, concat_axis=0, tiled=True)  21.6 us
    all_to_all x1, blocking collectives, shards(): lax.all_to_all(cotan_buf, 'sp', split_axis=0, concat_axis=0, tiled=True)  17.7 us
    dot_general x4, matrix products, contract_rows(): lax.dot_general(left, right, (((0,), (0,)), ((), ())), preferred_element_...  17.5 us
    all_gather x1, blocking collectives, shards(): full_stream = lax.all_gather(stream, 'tp', axis=1, tiled=True)  10.2 us
    psum x1, blocking collectives, shards(): lax.psum((jnp.sum(norm_grad, axis=1), jnp.sum(norm_grad * normed, axis=1)...  8.9 us
    all_to_all x1, waiting for transfers between devices, shards(): lax.all_to_all(row_share.reshape(experts, capacity, slice_width), 'sp', s...  8.7 us
  transfers between devices with their start and end apart: 6, of which 3 were waited for; matrix products, arithmetic and copies ran while one was open for 16% of the time, Pallas kernels for 0%

profile of v1, /device:TPU:0, one launch (start us, length us, event | category | flops | bytes accessed | tf_op | source)
XLA Modules:
  0.0 222.2 jit_solution(2536029228179971361)
XLA Ops:
  8.1 0.9 copy.31
  11.2 3.9 %scatter_custom_fusion.1 = bf16[512,512]{1,0:T(8,128)(2,1)S(1)} fusion(s32[256]{0:T(256)S(1)} %bitcast.130, bf16[128,512]{1,0:T(8,128)(2,1)} %param.15, s32[1024]{0:T(1024)S(1)} %pad_clamp_fusion.1, bf16[]{:T(256)} %constant.29.clone.1), kind=kCustom, calls=%fused_computation.94 | custom fusion | bytes 524800 | tf_op jit(solution)/shard_map/scatter | solution.py:67
  15.1 21.6 %all_to_all.20 = bf16[8,64,512]{2,1,0:T(8,128)(2,1)} all-to-all(bf16[8,64,512]{2,1,0:T(8,128)(2,1)S(1)} %bitcast.97), channel_id=1, replica_groups=mesh['sp'=8,'tp'=4] {'sp'}, dimensions={0} | all-to-all | bytes 1048576 | tf_op jit(solution)/shard_map/all_to_all | solution.py:74
  37.1 2.9 %scatter_custom_fusion = bf16[512,512]{1,0:T(8,128)(2,1)S(1)} fusion(s32[256]{0:T(256)S(1)} %bitcast.131, f32[256]{0:T(256)S(1)} %mul.427, bf16[]{:T(256)} %constant.29.clone.1, bf16[128,512]{1,0:T(8,128)(2,1)S(1)} %copy-done.4, s32[1024]{0:T(1024)S(1)} %pad_clamp_fusion.1), kind=kCustom, calls=%fused_computation.89 | custom fusion | flops 393216 | bytes 660482 | tf_op jit(solution)/shard_map/scatter | solution.py:68
  39.9 17.7 %all_to_all.21 = bf16[8,64,512]{2,1,0:T(8,128)(2,1)S(1)} all-to-all(bf16[8,64,512]{2,1,0:T(8,128)(2,1)S(1)} %bitcast.96), channel_id=1, replica_groups=mesh['sp'=8,'tp'=4] {'sp'}, dimensions={0} | all-to-all | bytes 1048576 | tf_op jit(solution)/shard_map/all_to_all | solution.py:75
  57.9 35.7 %all_to_all.22 = bf16[4,8,64,512]{3,2,1,0:T(8,128)(2,1)S(1)} all-to-all(bf16[4,8,64,512]{3,2,1,0:T(8,128)(2,1)S(1)} %stack.2), channel_id=1, replica_groups=mesh['sp'=8,'tp'=4] {'tp'}, dimensions={0} | all-to-all | bytes 4194304 | tf_op jit(solution)/shard_map/all_to_all | solution.py:9
  93.7 1.6 copy.34
  95.3 1.9 copy.39
  97.3 3.4 %fusion.5 = f32[512,704]{0,1:T(8,128)S(1)} fusion(bf16[512,2048]{1,0:T(8,128)(2,1)} %bitcast.135, bf16[1,704,2048]{2,1,0:T(8,128)(2,1)S(1)} %copy-done), kind=kOutput, calls=%fused_computation.14 | convolution fusion | flops 1476395008 | bytes 6422528 | tf_op jit(solution)/shard_map/dot_general | solution.py:35
  100.8 1.7 fusion.8
  102.8 1.4 copy-done.43
  104.2 2.1 multiply_convert_fusion.1
  106.4 1.9 fusion.3
  108.3 3.3 %add_convert_fusion = bf16[512,2048]{1,0:T(8,128)(2,1)} fusion(f32[512,2048]{1,0:T(8,128)S(1)} %fusion.3, bf16[512,704]{0,1:T(8,128)(2,1)S(1)} %get-tuple-element.13, bf16[1,704,2048]{2,1,0:T(8,128)(2,1)S(1)} %copy-done.44), kind=kOutput, calls=%fused_computation.5 | convolution fusion | flops 1478492160 | bytes 9895936 | tf_op jit(solution)/shard_map/dot_general | solution.py:100
  112.2 34.2 %reduce-scatter.3.cloned.1.call-done = bf16[512,512]{1,0:T(8,128)(2,1)} async-done(((bf16[512,2048]{1,0:T(8,128)(2,1)}), bf16[512,512]{1,0:T(8,128)(2,1)}) %reduce-scatter.3.cloned.1.call-update) | async-done | bytes 524304 | tf_op jit(solution)/shard_map/reduce_scatter | solution.py:103
  146.4 4.6 %all-to-all-start.3 = ((bf16[8,64,512]{2,1,0:T(8,128)(2,1)}), bf16[8,64,512]{2,1,0:T(8,128)(2,1)S(1)}, u32[]{:S(2)}, u32[]{:S(2)}) async-start(bf16[8,64,512]{2,1,0:T(8,128)(2,1)} %bitcast.98), calls=%async_computation.4 | async-start | bytes 1048576 | tf_op jit(solution)/shard_map/all_to_all | solution.py:107
  152.6 5.1 %fusion.1 = bf16[1,704,2048]{2,1,0:T(8,128)(2,1)} fusion(bf16[512,704]{0,1:T(8,128)(2,1)} %copy-done.46, bf16[512,2048]{1,0:T(8,128)(2,1)} %bitcast.136), kind=kOutput, calls=%fused_computation.10 | convolution fusion | flops 1477836800 | bytes 5701632 | tf_op jit(solution)/shard_map/dot_general | solution.py:29
  157.6 8.7 %all-to-all-done.3 = bf16[8,64,512]{2,1,0:T(8,128)(2,1)S(1)} async-done(((bf16[8,64,512]{2,1,0:T(8,128)(2,1)}), bf16[8,64,512]{2,1,0:T(8,128)(2,1)S(1)}, u32[]{:S(2)}, u32[]{:S(2)}) %all-to-all-start.3) | async-done | bytes 524320 | tf_op jit(solution)/shard_map/all_to_all | solution.py:107
  166.3 1.9 gather_fusion
  168.2 1.3 reshape.143
  169.9 1.0 fusion.18
  170.9 10.2 %all_gather.10 = bf16[128,2048]{1,0:T(8,128)(2,1)S(1)} all-gather(bf16[128,512]{1,0:T(8,128)(2,1)S(1)} %fusion.18), channel_id=1, replica_groups=mesh['sp'=8,'tp'=4] {'tp'}, dimensions={1}, use_global_device_ids=true | all-gather | bytes 655360 | tf_op jit(solution)/shard_map/all_gather | solution.py:120
  181.1 1.6 convolution_convert_fusion.3
  182.8 5.7 %fusion.2 = bf16[1,704,2048]{2,1,0:T(8,128)(2,1)} fusion(bf16[512,2048]{1,0:T(8,128)(2,1)} %bitcast.94, f32[512,704]{0,1:T(8,128)} %copy-done.48, f32[512,704]{0,1:T(8,128)} %copy-done.47), kind=kOutput, calls=%fused_computation.11 | convolution fusion | flops 1479999488 | bytes 7864320 | tf_op jit(solution)/shard_map/dot_general | solution.py:29
  188.5 2.3 %fusion.125 = (f32[128]{0:T(128)S(1)}, f32[128]{0:T(128)S(1)}, f32[128,256]{1,0:T(8,128)}) fusion(f32[128]{0:T(128)} %param.26, f32[128]{0:T(128)} %param.25, bf16[128,256]{1,0:T(8,128)(2,1)} %param.24, f32[256]{0:T(256)} %param.27, bf16[128,2048]{1,0:T(8,128)(2,1)S(1)} %all_gather.10, bf16[2048,256]{1,0:T(8,128)(2,1)} %all-gather.5.cloned.1.call-done), kind=kOutput, calls=%fused_computation.223 | convolution fusion | flops 134741760 | bytes 1772544 | tf_op jit(solution)/shard_map/dot_general | solution.py:126
  190.8 8.9 %all-reduce = (f32[128]{0:T(128)S(1)}, f32[128]{0:T(128)S(1)}) all-reduce(f32[128]{0:T(128)S(1)} %get-tuple-element.8, f32[128]{0:T(128)S(1)} %get-tuple-element.7), channel_id=1, replica_groups=mesh['sp'=8,'tp'=4] {'tp'}, use_global_device_ids=true, to_apply=%region_10.11 | all-reduce | flops 256 | bytes 2048 | tf_op jit(solution)/shard_map/psum | solution.py:137
  199.8 1.0 subtract_multiply_fusion
  201.1 1.3 collective-permute-start
  202.4 5.1 %fusion = bf16[1,704,2048]{2,1,0:T(8,128)(2,1)} fusion(bf16[512,704]{0,1:T(8,128)(2,1)} %copy-done.2, bf16[512,2048]{1,0:T(8,128)(2,1)} %bitcast.137), kind=kOutput, calls=%fused_computation.9 | convolution fusion | flops 1477836800 | bytes 5701632 | tf_op jit(solution)/shard_map/dot_general | solution.py:29
  207.8 1.1 multiply_convert_fusion.6
  209.6 3.6 %reduce-scatter.5.cloned.1.call-done = bf16[256,256]{1,0:T(8,128)(2,1)} async-done(((bf16[2048,256]{1,0:T(8,128)(2,1)}), bf16[256,256]{1,0:T(8,128)(2,1)}) %reduce-scatter.5.cloned.1.call-update) | async-done | bytes 131088 | tf_op jit(solution)/shard_map/reduce_scatter | solution.py:132
  213.2 1.6 convert_element_type.92
  (132 shorter events, 6.6 us)
Async XLA Ops:
  8.0 89.3 %copy-start = (bf16[1,704,2048]{2,1,0:T(8,128)(2,1)S(1)}, bf16[1,704,2048]{2,1,0:T(8,128)(2,1)}, u32[]{:S(2)}) copy-start(bf16[1,704,2048]{2,1,0:T(8,128)(2,1)} %param.19) | copy-start | bytes 8650756
  8.0 28.8 %copy-start.41 = (f32[128,2]{0,1:T(2,128)S(1)}, f32[128,2]{0,1:T(2,128)}, u32[]{:S(2)}) copy-start(f32[128,2]{0,1:T(2,128)} %param.18) | copy-start | bytes 3076
  8.0 29.0 %copy-start.4 = (bf16[128,512]{1,0:T(8,128)(2,1)S(1)}, bf16[128,512]{1,0:T(8,128)(2,1)}, u32[]{:S(2)}) copy-start(bf16[128,512]{1,0:T(8,128)(2,1)} %param.16) | copy-start | bytes 393220
  8.0 89.2 %all-gather.3.cloned.1.call-start = ((), (), s32[]{:S(2)}) async-start(), calls=%async_computation.6 | async-start | bytes 2621440 | tf_op jit(solution)/shard_map/all_gather | solution.py:78
  36.7 109.7 %reduce-scatter.3.cloned.1.call-start = ((), (), s32[]{:S(2)}) async-start(), calls=%async_computation.7 | async-start | bytes 2621440 | tf_op jit(solution)/shard_map/reduce_scatter | solution.py:103
  111.6 39.7 %copy-start.9 = (bf16[31,256]{1,0:T(8,128)(2,1)S(1)}, bf16[31,256]{1,0:T(8,128)(2,1)}, u32[]{:S(2)}) copy-start(bf16[31,256]{1,0:T(8,128)(2,1)} %param.28) | copy-start | bytes 47620
  111.6 76.9 %all-gather.5.cloned.1.call-start = ((), (), s32[]{:S(2)}) async-start(), calls=%async_computation.9 | async-start | bytes 1179648 | tf_op jit(solution)/shard_map/all_gather | solution.py:128
  146.4 19.9 %all-to-all-start.3 = ((bf16[8,64,512]{2,1,0:T(8,128)(2,1)}), bf16[8,64,512]{2,1,0:T(8,128)(2,1)S(1)}, u32[]{:S(2)}, u32[]{:S(2)}) async-start(bf16[8,64,512]{2,1,0:T(8,128)(2,1)} %bitcast.98), calls=%async_computation.4 | async-start | bytes 1048576 | tf_op jit(solution)/shard_map/all_to_all | solution.py:107
  151.0 62.2 %reduce-scatter.5.cloned.1.call-start = ((), (), s32[]{:S(2)}) async-start(), calls=%async_computation.8 | async-start | bytes 1179648 | tf_op jit(solution)/shard_map/reduce_scatter | solution.py:132
  169.5 11.6 %copy-start.5 = (bf16[128,256]{1,0:T(8,128)(2,1)S(1)}, bf16[128,256]{1,0:T(8,128)(2,1)}, u32[]{:S(2)}) copy-start(bf16[128,256]{1,0:T(8,128)(2,1)} %param.24) | copy-start | bytes 196612
  169.5 11.6 %copy-start.37 = (f32[128]{0:T(128)S(1)}, f32[128]{0:T(128)}, u32[]{:S(2)}) copy-start(f32[128]{0:T(128)} %param.26) | copy-start | bytes 1540
  169.5 11.6 %copy-start.39 = (f32[128]{0:T(128)S(1)}, f32[128]{0:T(128)}, u32[]{:S(2)}) copy-start(f32[128]{0:T(128)} %param.25) | copy-start | bytes 1540
  169.5 11.6 %copy-start.42 = (f32[256]{0:T(256)S(1)}, f32[256]{0:T(256)}, u32[]{:S(2)}) copy-start(f32[256]{0:T(256)} %param.27) | copy-start | bytes 3076
  170.9 17.6 %copy-start.3 = (bf16[128,512]{1,0:T(8,128)(2,1)}, bf16[128,512]{1,0:T(8,128)(2,1)S(1)}, u32[]{:S(2)}) copy-start(bf16[128,512]{1,0:T(8,128)(2,1)S(1)} %fusion.18) | copy-start | bytes 393220
  188.5 11.2 %copy-start.6 = (bf16[128,256]{1,0:T(8,128)(2,1)S(1)}, bf16[128,256]{1,0:T(8,128)(2,1)}, u32[]{:S(2)}) copy-start(bf16[128,256]{1,0:T(8,128)(2,1)} %param.24) | copy-start | bytes 196612
  188.5 11.2 %copy-start.38 = (f32[128]{0:T(128)S(1)}, f32[128]{0:T(128)}, u32[]{:S(2)}) copy-start(f32[128]{0:T(128)} %param.26) | copy-start | bytes 1540
  188.5 11.2 %copy-start.40 = (f32[128]{0:T(128)S(1)}, f32[128]{0:T(128)}, u32[]{:S(2)}) copy-start(f32[128]{0:T(128)} %param.25) | copy-start | bytes 1540
  200.8 6.7 %copy-start.7 = (bf16[128,256]{1,0:T(8,128)(2,1)S(1)}, bf16[128,256]{1,0:T(8,128)(2,1)}, u32[]{:S(2)}) copy-start(bf16[128,256]{1,0:T(8,128)(2,1)} %param.23) | copy-start | bytes 196612
  200.8 6.7 %copy-start.8 = (bf16[128,256]{1,0:T(8,128)(2,1)S(1)}, bf16[128,256]{1,0:T(8,128)(2,1)}, u32[]{:S(2)}) copy-start(bf16[128,256]{1,0:T(8,128)(2,1)} %param.22) | copy-start | bytes 196612
  200.8 6.7 %copy-start.10 = (f32[1,256]{1,0:T(1,128)S(1)}, f32[1,256]{1,0:T(1,128)}, u32[]{:S(2)}) copy-start(f32[1,256]{1,0:T(1,128)} %get-tuple-element.40) | copy-start | bytes 3076
  200.9 6.7 %copy-start.11 = (f32[1,256]{1,0:T(1,128)S(1)}, f32[1,256]{1,0:T(1,128)}, u32[]{:S(2)}) copy-start(f32[1,256]{1,0:T(1,128)} %get-tuple-element.41) | copy-start | bytes 3076
  200.9 6.7 %copy-start.12 = (f32[1,256]{1,0:T(1,128)S(1)}, f32[1,256]{1,0:T(1,128)}, u32[]{:S(2)}) copy-start(f32[1,256]{1,0:T(1,128)} %get-tuple-element.42) | copy-start | bytes 3076
  200.9 6.7 %copy-start.13 = (f32[1,256]{1,0:T(1,128)S(1)}, f32[1,256]{1,0:T(1,128)}, u32[]{:S(2)}) copy-start(f32[1,256]{1,0:T(1,128)} %get-tuple-element.43) | copy-start | bytes 3076
  200.9 6.7 %copy-start.14 = (f32[1,256]{1,0:T(1,128)S(1)}, f32[1,256]{1,0:T(1,128)}, u32[]{:S(2)}) copy-start(f32[1,256]{1,0:T(1,128)} %get-tuple-element.44) | copy-start | bytes 3076
  200.9 6.7 %copy-start.15 = (f32[1,256]{1,0:T(1,128)S(1)}, f32[1,256]{1,0:T(1,128)}, u32[]{:S(2)}) copy-start(f32[1,256]{1,0:T(1,128)} %get-tuple-element.45) | copy-start | bytes 3076
  200.9 6.7 %copy-start.16 = (f32[1,256]{1,0:T(1,128)S(1)}, f32[1,256]{1,0:T(1,128)}, u32[]{:S(2)}) copy-start(f32[1,256]{1,0:T(1,128)} %get-tuple-element.46) | copy-start | bytes 3076
  200.9 6.7 %copy-start.17 = (f32[1,256]{1,0:T(1,128)S(1)}, f32[1,256]{1,0:T(1,128)}, u32[]{:S(2)}) copy-start(f32[1,256]{1,0:T(1,128)} %get-tuple-element.47) | copy-start | bytes 3076
  200.9 6.7 %copy-start.18 = (f32[1,256]{1,0:T(1,128)S(1)}, f32[1,256]{1,0:T(1,128)}, u32[]{:S(2)}) copy-start(f32[1,256]{1,0:T(1,128)} %get-tuple-element.17) | copy-start | bytes 3076
  200.9 6.7 %copy-start.19 = (f32[1,256]{1,0:T(1,128)S(1)}, f32[1,256]{1,0:T(1,128)}, u32[]{:S(2)}) copy-start(f32[1,256]{1,0:T(1,128)} %get-tuple-element.18) | copy-start | bytes 3076
  201.0 6.7 %copy-start.20 = (f32[1,256]{1,0:T(1,128)S(1)}, f32[1,256]{1,0:T(1,128)}, u32[]{:S(2)}) copy-start(f32[1,256]{1,0:T(1,128)} %get-tuple-element.19) | copy-start | bytes 3076
  201.0 6.7 %copy-start.21 = (f32[1,256]{1,0:T(1,128)S(1)}, f32[1,256]{1,0:T(1,128)}, u32[]{:S(2)}) copy-start(f32[1,256]{1,0:T(1,128)} %get-tuple-element.20) | copy-start | bytes 3076
  201.1 6.4 %collective-permute-start = (f32[30,256]{1,0:T(8,128)S(1)}, f32[30,256]{1,0:T(8,128)S(1)}, u32[]{:S(2)}, u32[]{:S(2)}) collective-permute-start(f32[30,256]{1,0:T(8,128)S(1)} %slice.274), channel_id=1, source_target_pairs={{4,0},{8,4},{12,8},{16,12},{20,16},{24,20},{28,24},{5,1},{9,5},{13... | collective-permute-start | bytes 92168 | tf_op jit(solution)/shard_map/ppermute | solution.py:15
  (23 other events, 121.7 us)
Sparse Core Ops, SparseCore 0:
  36.9 47.4 all-gather.2
  111.7 34.6 reduce-scatter.2
Sparse Core Ops, SparseCore 1:
  113.7 21.6 all-gather.4
  182.9 30.3 reduce-scatter.4
